TPU v7x, 32 devices: a whole 2x2x4 slice. The times are simulated.
32 devices in a mesh: sp: 4 (over z), tp: 4 (over y, x), dp: 2 (over core).
Axes of the slice: x: 2, y: 2, z: 4, core: 2. Of those that a mesh axis runs over, the one named last changes fastest.
Arguments:
- latent: bfloat16 [2, 512, 2048], P('dp', ('sp', 'tp')), may hold values from -10 to 10
- condition: bfloat16 [2, 2048], P('dp'), may hold values from -6 to 6
- context: bfloat16 [2, 512, 2048], P('dp', 'sp'), may hold values from -6 to 6
- context_source: bfloat16 [2048], replicated, may hold values from -6 to 6
- mod_weight: bfloat16 [3, 2048, 2048], P(None, 'sp', 'tp'), may hold values from -0.125 to 0.125
- norm_gain: bfloat16 [2048], replicated, may hold values from 0.099609375 to 1.8984375
- w_x: bfloat16 [2048, 2048], P('dp', 'tp'), may hold values from -0.125 to 0.125
- w_b: bfloat16 [2048, 512], P('dp', 'tp'), may hold values from -0.125 to 0.125
- w_c: bfloat16 [2048, 512], P('dp', 'tp'), may hold values from -0.125 to 0.125
- w_z: bfloat16 [2048, 2048], P('dp', 'tp'), may hold values from -0.125 to 0.125
- w_dt: bfloat16 [2, 2048, 32], P(None, 'dp', 'tp'), may hold values from -0.125 to 0.125
- conv_x: bfloat16 [3, 2048], P(None, 'tp'), may hold values from -3.5 to 3.5
- conv_b: bfloat16 [3, 512], P(None, 'tp'), may hold values from -3.5 to 3.5
- conv_c: bfloat16 [3, 512], P(None, 'tp'), may hold values from -3.5 to 3.5
- decay_rate: float32 [2, 32], P(None, 'tp'), may hold values from 0 to 1, as said below
- out_gain: bfloat16 [2048], P('tp'), may hold values from 0.099609375 to 1.8984375
- w_out: bfloat16 [2048, 2048], P(('tp', 'dp')), may hold values from -0.125 to 0.125
Outputs:
- update: bfloat16 [2, 512, 2048], P('dp', ('sp', 'tp'))
Inputs may be any that keep to these rules, and one draw needn't show every extreme that they name: `decay_rate`: positive rates.
All inputs are finite; a program needn't handle non-finite values.
Results may differ from a plain program's by a relative error of at most 0.014.
Values may be sent and summed in bfloat16 or wider, within the bound.
A program may use at most 128 MiB of HBM per device.

v0:
```python
import jax
import jax.numpy as jnp
from jax import lax
from jax.sharding import PartitionSpec as P

STATE = 128
BLOCK = 128
EPSILON = 1e-06


def with_halo(x, sides, width):
    for axis, dim in sides:
        peers, length = (lax.axis_size(axis), x.shape[dim])
        up = [(i, (i + 1) % peers) for i in range(peers - 1)]
        down = [(j, i) for i, j in up]
        last = lax.slice_in_dim(x, length - width, length, axis=dim)
        leading = lax.slice_in_dim(x, 0, width, axis=dim)
        before = lax.ppermute(last, axis, up)
        after = lax.ppermute(leading, axis, down)
        x = jnp.concatenate([before, x, after], axis=dim)
    return x


def carried_in_2(x, axis, combine, identity, reverse):
    peers, place = (lax.axis_size(axis), lax.axis_index(axis))
    everything = jax.tree.map(
        lambda part, kind: lax.all_gather(part.astype(kind), axis), x, (jnp.bfloat16, jnp.bfloat16)
    )
    start = jax.tree.map(
        lambda part, zero: jnp.broadcast_to(jnp.asarray(zero, part.dtype), part.shape), x, identity
    )

    def hop(k, before):
        at = peers - 1 - k if reverse else k
        reached = at > place if reverse else at < place
        new = combine(
            before, jax.tree.map(lambda part, own: part[at].astype(own.dtype), everything, x)
        )
        return jax.tree.map(lambda a, b: jnp.where(reached, a, b), new, before)

    return lax.fori_loop(0, peers, hop, start)


def rounded(values):
    return lax.optimization_barrier(values.astype(jnp.bfloat16)).astype(jnp.float32)


def modulated(source, gain_vec, shift_vec, scale_vec):
    values = source.astype(jnp.float32)
    normed = values * lax.rsqrt(jnp.mean(values * values, axis=-1, keepdims=True) + EPSILON)
    return (normed * gain_vec.astype(jnp.float32) * (1.0 + scale_vec) + shift_vec).astype(
        jnp.bfloat16
    )


def convolved(padded, weight, total_rows):
    wide_vals = padded.astype(jnp.float32)
    tap_weights = weight.astype(jnp.float32)
    summed = jnp.zeros((total_rows, wide_vals.shape[1]), jnp.float32)
    for offset in range(weight.shape[0]):
        summed = summed + wide_vals[offset : offset + total_rows] * tap_weights[offset]
    return jax.nn.silu(summed).astype(jnp.bfloat16)


def final_state(x_vals, b_vals, step_size, rate_head, groups):
    total_rows, head_count = step_size.shape
    per_group = head_count // groups
    moved_x = rounded(
        x_vals.reshape(total_rows, head_count, -1).astype(jnp.float32) * step_size[:, :, None]
    )
    running = jnp.cumsum(-rate_head * step_size, axis=0)
    weight = jnp.exp(running[-1:] - running)
    scaled = (moved_x * weight[:, :, None]).reshape(total_rows, groups, per_group, -1)
    b_wide = b_vals.reshape(total_rows, groups, -1).astype(jnp.float32)
    ctx_state = jnp.einsum("sgn,sghp->ghpn", b_wide, scaled, precision=lax.Precision.HIGHEST)
    return (ctx_state, running[-1].reshape(groups, per_group))


def combine_states(earlier, later_part):
    return (
        earlier[0] + later_part[0],
        earlier[1] * jnp.exp(later_part[0])[:, :, None, None] + later_part[1],
    )


def direction_terms(x_vals, b_vals, c_vals, step_size, rate_head, groups):
    total_rows, head_count = step_size.shape
    per_group = head_count // groups
    blocks = total_rows // BLOCK
    moved_x = (
        x_vals.reshape(total_rows, head_count, -1).astype(jnp.float32) * step_size[:, :, None]
    ).astype(jnp.bfloat16)
    head_dim = moved_x.shape[2]
    x_blocks = moved_x.reshape(blocks, BLOCK, groups, per_group, head_dim)
    b_blocks = b_vals.reshape(blocks, BLOCK, groups, -1)
    c_blocks = c_vals.reshape(blocks, BLOCK, groups, -1)
    running = jnp.cumsum((-rate_head * step_size).reshape(blocks, BLOCK, head_count), axis=1)
    across = jnp.swapaxes(running, 1, 2)
    spread = across[:, :, :, None] - across[:, :, None, :]
    lower_part = lax.broadcasted_iota(jnp.int32, (BLOCK, BLOCK), 0) >= lax.broadcasted_iota(
        jnp.int32, (BLOCK, BLOCK), 1
    )
    decay_mask = jnp.where(lower_part, jnp.exp(jnp.minimum(spread, 0.0)), 0.0).reshape(
        blocks, groups, per_group, BLOCK, BLOCK
    )
    scores = jnp.einsum("clgn,csgn->cgls", c_blocks, b_blocks, preferred_element_type=jnp.float32)
    weights = (scores[:, :, None] * decay_mask).astype(jnp.bfloat16)
    inside = jnp.einsum("cghls,csghp->clghp", weights, x_blocks, preferred_element_type=jnp.float32)
    to_end = jnp.exp(running[:, -1:, :] - running).reshape(blocks, BLOCK, groups, per_group, 1)
    x_end = (x_blocks.astype(jnp.float32) * to_end).astype(jnp.bfloat16)
    fresh_state = jnp.einsum(
        "csgn,csghp->cghpn", b_blocks, x_end, preferred_element_type=jnp.float32
    )
    totals = running[:, -1, :].reshape(blocks, groups, per_group)

    def advance(carried_in, inputs):
        return (carried_in * jnp.exp(inputs[1])[:, :, None, None] + inputs[0], carried_in)

    ending, before = lax.scan(
        advance, jnp.zeros(fresh_state.shape[1:], jnp.float32), (fresh_state, totals)
    )
    return (inside, before, ending, totals, running, c_blocks)


def direction_output(terms, incoming):
    inside, before, ending, totals, running, c_blocks = terms
    blocks, length, groups, per_group, head_dim = inside.shape
    offset_sum = jnp.cumsum(totals, axis=0) - totals
    entering = before + jnp.exp(offset_sum)[:, :, :, None, None] * incoming[None]
    carried = jnp.einsum(
        "clgn,cghpn->clghp",
        c_blocks,
        entering.astype(jnp.bfloat16),
        preferred_element_type=jnp.float32,
    )
    growth = jnp.exp(running).reshape(blocks, length, groups, per_group, 1)
    return (inside + growth * carried).reshape(blocks * length, -1)


def shards(
    latent,
    condition,
    context,
    context_source,
    mod_weight,
    norm_gain,
    w_x,
    w_b,
    w_c,
    w_z,
    w_dt,
    conv_x,
    conv_b,
    conv_c,
    decay_rate,
    out_gain,
    w_out,
):
    row_count = mod_weight.shape[1]
    activations = jnp.stack(
        [
            jax.nn.silu(condition[0].astype(jnp.float32)),
            jax.nn.silu(context_source.astype(jnp.float32)),
        ]
    ).astype(jnp.bfloat16)
    own_rows = lax.dynamic_slice_in_dim(activations, lax.axis_index("sp") * row_count, row_count, 1)
    partial_value = jnp.einsum(
        "ar,krc->kac", own_rows, mod_weight, preferred_element_type=jnp.float32
    )
    summed = lax.psum(partial_value, "sp")
    mod_vectors = lax.all_gather(summed, "tp", axis=2, tiled=True)
    full_x, full_b, full_c, full_z, full_fwd, full_bwd, full_out = (
        lax.all_gather(w_x, "dp", axis=0, tiled=True),
        lax.all_gather(w_b, "dp", axis=0, tiled=True),
        lax.all_gather(w_c, "dp", axis=0, tiled=True),
        lax.all_gather(w_z, "dp", axis=0, tiled=True),
        lax.all_gather(w_dt[0], "dp", axis=0, tiled=True),
        lax.all_gather(w_dt[1], "dp", axis=0, tiled=True),
        lax.all_gather(w_out, "dp", axis=0, tiled=True),
    )
    inner_cols = full_x.shape[1]
    gn_cols = full_b.shape[1]
    head_count = full_fwd.shape[1]
    groups = gn_cols // STATE
    mixed_cols = inner_cols + gn_cols
    reach_rows = conv_x.shape[0] // 2
    rate_fwd = decay_rate[0]
    rate_bwd = decay_rate[1]
    all_weights = jnp.concatenate([full_x, full_b, full_c, full_fwd, full_bwd, full_z], axis=1)
    ctx_weight = jnp.concatenate([full_x, full_b, full_fwd, full_bwd], axis=1)
    taps_all = jnp.concatenate([conv_x, conv_b, conv_c], axis=1)
    ctx_taps = jnp.concatenate([conv_x, conv_b], axis=1)
    ctx_rows = modulated(context[0], norm_gain, mod_vectors[0, 1], mod_vectors[1, 1])
    own_features = jnp.dot(ctx_rows, ctx_weight, preferred_element_type=jnp.float32).astype(
        jnp.bfloat16
    )
    own_count = own_features.shape[0]
    padded = with_halo(own_features[:, :mixed_cols], (("sp", 0),), reach_rows)
    smoothed = convolved(padded, ctx_taps, own_count)
    step_size = jax.nn.softplus(own_features[:, mixed_cols:].astype(jnp.float32))
    ctx_x = smoothed[:, :inner_cols]
    ctx_b = smoothed[:, inner_cols:]
    part_fwd, total_fwd = final_state(ctx_x, ctx_b, step_size[:, :head_count], rate_fwd, groups)
    part_bwd, total_bwd = final_state(
        jnp.flip(ctx_x, 0),
        jnp.flip(ctx_b, 0),
        jnp.flip(step_size[:, head_count:], 0),
        rate_bwd,
        groups,
    )
    totals = lax.all_gather(jnp.stack([total_fwd, total_bwd])[None], "sp", axis=0, tiled=True)
    device_order = jnp.arange(totals.shape[0])
    own_index = lax.axis_index("sp")
    after_sum = jnp.sum(
        jnp.where((device_order > own_index)[:, None, None], totals[:, 0], 0.0), axis=0
    )
    before_sum = jnp.sum(
        jnp.where((device_order < own_index)[:, None, None], totals[:, 1], 0.0), axis=0
    )
    ctx_fwd, ctx_bwd = lax.psum(
        (
            part_fwd * jnp.exp(after_sum)[:, :, None, None],
            part_bwd * jnp.exp(before_sum)[:, :, None, None],
        ),
        "sp",
    )
    latent_rows = modulated(latent[0], norm_gain, mod_vectors[0, 0], mod_vectors[1, 0])
    features = jnp.dot(
        lax.all_gather(latent_rows, "tp", axis=0, tiled=True),
        all_weights,
        preferred_element_type=jnp.float32,
    ).astype(jnp.bfloat16)
    total_rows = features.shape[0]
    padded = with_halo(features[:, : mixed_cols + gn_cols], (("sp", 0),), reach_rows)
    smoothed = convolved(padded, taps_all, total_rows)
    x_vals = smoothed[:, :inner_cols]
    b_vals = smoothed[:, inner_cols:mixed_cols]
    c_vals = smoothed[:, mixed_cols:]
    base_col = mixed_cols + gn_cols
    step_size = jax.nn.softplus(
        features[:, base_col : base_col + 2 * head_count].astype(jnp.float32)
    )
    gate_in = features[:, base_col + 2 * head_count :]
    forward_terms = direction_terms(
        x_vals, b_vals, c_vals, step_size[:, :head_count], rate_fwd, groups
    )
    backward_terms = direction_terms(
        jnp.flip(x_vals, 0),
        jnp.flip(b_vals, 0),
        jnp.flip(c_vals, 0),
        jnp.flip(step_size[:, head_count:], 0),
        rate_bwd,
        groups,
    )
    fwd_total = jnp.sum(forward_terms[3], axis=0)
    bwd_total = jnp.sum(backward_terms[3], axis=0)
    empty = (jnp.zeros_like(fwd_total), jnp.zeros_like(forward_terms[2]))
    prefix_decay, prefix_state = carried_in_2(
        (fwd_total, forward_terms[2]), "sp", combine_states, empty, False
    )
    suffix_decay, suffix_state = carried_in_2(
        (bwd_total, backward_terms[2]), "sp", combine_states, empty, True
    )
    out_fwd = direction_output(
        forward_terms, prefix_state + jnp.exp(prefix_decay)[:, :, None, None] * ctx_fwd
    )
    out_bwd = jnp.flip(
        direction_output(
            backward_terms, suffix_state + jnp.exp(suffix_decay)[:, :, None, None] * ctx_bwd
        ),
        0,
    )
    gated = (out_fwd + out_bwd) * jax.nn.silu(gate_in.astype(jnp.float32))
    grouped = gated.reshape(total_rows, groups, -1)
    normed = (
        grouped
        * lax.rsqrt(jnp.mean(grouped * grouped, axis=-1, keepdims=True) + EPSILON)
        * out_gain.reshape(groups, -1).astype(jnp.float32)
    )
    normed_out = normed.reshape(total_rows, -1).astype(jnp.bfloat16)
    mixed = lax.psum_scatter(
        jnp.dot(normed_out, full_out, preferred_element_type=jnp.float32).astype(jnp.bfloat16),
        "tp",
        scatter_dimension=0,
        tiled=True,
    ).astype(jnp.float32)
    return (mod_vectors[2, 0] * mixed).astype(jnp.bfloat16)[None]


def solution(mesh):
    placed = (
        P("dp", ("sp", "tp"), None),
        P("dp", None),
        P("dp", "sp", None),
        P(),
        P(None, "sp", "tp"),
        P(),
        P("dp", "tp"),
        P("dp", "tp"),
        P("dp", "tp"),
        P("dp", "tp"),
        P(None, "dp", "tp"),
        P(None, "tp"),
        P(None, "tp"),
        P(None, "tp"),
        P(None, "tp"),
        P("tp"),
        P(("tp", "dp"), None),
    )
    return jax.shard_map(
        shards, mesh=mesh, in_specs=placed, out_specs=P("dp", ("sp", "tp"), None), check_vma=False
    )
```

profile of v0, /device:TPU:0, one launch (start us, length us, event | category | flops | bytes accessed | tf_op | source)
XLA Modules:
  0.0 216.8 jit_solution(12759376264633219292)
XLA Ops:
  9.9 20.4 %psum.21 = f32[3,2,512]{2,1,0:T(2,128)S(1)} all-reduce(f32[3,2,512]{2,1,0:T(2,128)S(1)} %convolution_bitcast_fusion.4), channel_id=1, replica_groups=mesh['sp'=4,'tp'=4,'dp'=2] {'sp'}, use_global_device_ids=true, to_apply=%region_0.1 | all-reduce | flops 3072 | bytes 24576 | tf_op jit(solution)/shard_map/psum | solution.py:170
  30.4 8.3 %all_gather.50 = f32[3,2,2048]{2,1,0:T(2,128)S(1)} all-gather(f32[3,2,512]{2,1,0:T(2,128)S(1)} %psum.21), channel_id=1, replica_groups=mesh['sp'=4,'tp'=4,'dp'=2] {'tp'}, dimensions={2}, use_global_device_ids=true | all-gather | bytes 61440 | tf_op jit(solution)/shard_map/all_gather | solution.py:171
  39.1 1.8 all-gather
  41.2 1.8 all-gather.1
  43.3 10.0 %all_gather.51 = bf16[128,2048]{1,0:T(8,128)(2,1)S(1)} all-gather(bf16[32,2048]{1,0:T(8,128)(2,1)S(1)} %fusion.46), channel_id=1, replica_groups=mesh['sp'=4,'tp'=4,'dp'=2] {'tp'}, dimensions={0}, use_global_device_ids=true | all-gather | bytes 655360 | tf_op jit(solution)/shard_map/all_gather | solution.py:229
  53.9 3.8 %all_gather.53 = bf16[2048,128]{1,0:T(8,128)(2,1)} all-gather(bf16[1024,128]{1,0:T(8,128)(2,1)} %param.28), channel_id=1, replica_groups=mesh['sp'=4,'tp'=4,'dp'=2] {'dp'}, dimensions={0}, use_global_device_ids=true | all-gather | bytes 786432 | tf_op jit(solution)/shard_map/all_gather | solution.py:174
  57.7 4.1 %all_gather.54 = bf16[2048,128]{1,0:T(8,128)(2,1)} all-gather(bf16[1024,128]{1,0:T(8,128)(2,1)} %param.29), channel_id=1, replica_groups=mesh['sp'=4,'tp'=4,'dp'=2] {'dp'}, dimensions={0}, use_global_device_ids=true | all-gather | bytes 786432 | tf_op jit(solution)/shard_map/all_gather | solution.py:175
  61.8 1.2 fusion.23
  63.0 3.5 %fusion.16 = bf16[128,656]{0,1:T(8,128)(2,1)S(1)} fusion(bf16[2048,8]{1,0:T(8,128)(2,1)S(1)} %copy.71, bf16[2048,8]{1,0:T(8,128)(2,1)S(1)} %copy.70, bf16[2048,128]{1,0:T(8,128)(2,1)} %all_gather.53, bf16[2048,512]{1,0:T(8,128)(2,1)} %all-gather.9.cloned.1.call-done, bf16[1,128,2048]{2,1,0:T(8,128)(2,1)} %param.23, f32[2048]{0:T(1024)S(1)} %bitcast.220, ...), kind=kOutput, calls=%fused_computation.38 | convolution fusion | flops 356337664 | bytes 3404288 | tf_op jit(solution)/shard_map/dot_general | solution.py:194
  67.4 10.2 %concatenate.18 = bf16[2048,1296]{1,0:T(8,128)(2,1)} concatenate(bf16[2048,512]{1,0:T(8,128)(2,1)} %all-gather.9.cloned.1.call-done, bf16[2048,128]{1,0:T(8,128)(2,1)} %all_gather.53, bf16[2048,128]{1,0:T(8,128)(2,1)} %all_gather.54, bf16[2048,8]{1,0:T(8,128)(2,1)S(1)} %copy.70, bf16[2048,8]{1,0:T(8,128)(2,1)S(1)} %copy.71, bf16[2048,512]{1,0:T(8,128)(2,1)} %all-gather.11.cloned.1.call-done), dimensions={1} | concatenate | bytes 10616832 | tf_op jit(solution)/shard_map/concatenate | solution.py:189
  77.6 5.0 %convolution_convert_fusion.1 = bf16[128,1296]{0,1:T(8,128)(2,1)S(1)} fusion(bf16[128,2048]{1,0:T(8,128)(2,1)S(1)} %all_gather.51, bf16[2048,1296]{1,0:T(8,128)(2,1)} %concatenate.18), kind=kOutput, calls=%fused_computation.23 | convolution fusion | flops 679643136 | bytes 6164480 | tf_op jit(solution)/shard_map/dot_general | solution.py:228
  84.0 7.6 %all-gather.3 = f32[8,1,8]{2,1,0:T(1,128)S(1)} all-gather(f32[2,1,8]{2,1,0:T(1,128)S(1)} %pad_maximum_fusion.3), channel_id=5, replica_groups=mesh['sp'=4,'tp'=4,'dp'=2] {'sp'}, dimensions={0}, use_global_device_ids=true | all-gather | bytes 320 | tf_op jit(solution)/shard_map/all_gather | solution.py:211
  91.7 3.9 %collective-permute-start.2 = (bf16[1,640]{0,1:T(8,128)(2,1)S(1)}, bf16[1,640]{0,1:T(8,128)(2,1)S(1)}, u32[]{:S(2)}, u32[]{:S(2)}) collective-permute-start(bf16[1,640]{0,1:T(8,128)(2,1)S(1)} %copy-done.5), channel_id=1, source_target_pairs={{0,8},{8,16},{16,24},{1,9},{9,17},{17,25},{2,10},{10,18},{18,26},{... | collective-permute-start | bytes 3848 | tf_op jit(solution)/shard_map/ppermute | solution.py:18
  95.6 1.3 collective-permute-start.3
  97.2 1.1 collective-permute-done.2
  98.4 4.4 %collective-permute-done.3 = bf16[1,640]{0,1:T(8,128)(2,1)S(1)} collective-permute-done((bf16[1,640]{0,1:T(8,128)(2,1)S(1)}, bf16[1,640]{0,1:T(8,128)(2,1)S(1)}, u32[]{:S(2)}, u32[]{:S(2)}) %collective-permute-start.3) | collective-permute-done | bytes 1312 | tf_op jit(solution)/shard_map/ppermute | solution.py:19
  104.1 1.0 fusion.14
  105.1 1.0 fusion.12
  111.0 1.9 collective-permute-start
  113.0 1.3 collective-permute-start.1
  116.1 11.0 %all_gather.58 = bf16[4,1,8]{2,1,0:T(2,128)(2,1)} all-gather(bf16[1,1,8]{2,1,0:T(2,128)(2,1)S(1)} %slice.299), channel_id=1, replica_groups=mesh['sp'=4,'tp'=4,'dp'=2] {'sp'}, dimensions={0}, use_global_device_ids=true | all-gather | bytes 80 | tf_op jit(solution)/shard_map/all_gather | solution.py:27
  127.2 10.0 %all_gather.62 = bf16[4,1,8]{2,1,0:T(2,128)(2,1)} all-gather(bf16[1,1,8]{2,1,0:T(2,128)(2,1)S(1)} %slice.298), channel_id=1, replica_groups=mesh['sp'=4,'tp'=4,'dp'=2] {'sp'}, dimensions={0}, use_global_device_ids=true | all-gather | bytes 80 | tf_op jit(solution)/shard_map/all_gather | solution.py:27
  138.8 1.3 multiply_convert_fusion.2
  141.1 15.0 %all-gather.2 = bf16[32,64,128]{2,1,0:T(8,128)(2,1)S(1)} all-gather(bf16[8,64,128]{2,1,0:T(8,128)(2,1)S(1)} %fusion.21), channel_id=4, replica_groups=mesh['sp'=4,'tp'=4,'dp'=2] {'sp'}, dimensions={0}, use_global_device_ids=true | all-gather | bytes 655360 | tf_op jit(solution)/shard_map/all_gather | solution.py:27
  158.3 15.8 %all-gather.4 = bf16[32,64,128]{2,1,0:T(8,128)(2,1)S(1)} all-gather(bf16[8,64,128]{2,1,0:T(8,128)(2,1)S(1)} %fusion.22), channel_id=6, replica_groups=mesh['sp'=4,'tp'=4,'dp'=2] {'sp'}, dimensions={0}, use_global_device_ids=true | all-gather | bytes 655360 | tf_op jit(solution)/shard_map/all_gather | solution.py:27
  176.4 1.2 fusion.20
  177.6 1.2 fusion.13
  179.2 1.2 fusion.19
  180.4 1.2 fusion.15
  181.8 3.0 %convolution_convert_fusion = bf16[128,2048]{1,0:T(8,128)(2,1)} fusion(bf16[512,2048]{1,0:T(8,128)(2,1)} %all-gather.13.cloned.1.call-done, f32[128,512]{0,1:T(8,128)S(1)} %get-tuple-element.415, f32[512]{0:T(512)} %convert_element_type.388, f32[128]{0:T(128)S(1)} %add_rsqrt_fusion), kind=kOutput, calls=%fused_computation.22 | convolution fusion | flops 268894208 | bytes 2886144 | tf_op jit(solution)/shard_map/dot_general | solution.py:282
  184.8 23.9 %reduce-scatter.2.cloned.1.call-done = bf16[32,2048]{1,0:T(8,128)(2,1)} async-done(((bf16[128,2048]{1,0:T(8,128)(2,1)}), bf16[32,2048]{1,0:T(8,128)(2,1)}) %reduce-scatter.2.cloned.1.call-update) | async-done | bytes 131088 | tf_op jit(solution)/shard_map/reduce_scatter | solution.py:281
  208.7 1.6 fusion.71
  (183 shorter events, 23.9 us)
Async XLA Ops:
  6.5 3.0 %copy-start = (bf16[3,512,512]{2,1,0:T(8,128)(2,1)S(1)}, bf16[3,512,512]{2,1,0:T(8,128)(2,1)}, u32[]{:S(2)}) copy-start(bf16[3,512,512]{2,1,0:T(8,128)(2,1)} %param.25) | copy-start | bytes 4718596
  6.5 32.2 %copy-start.16 = (bf16[2048]{0:T(1024)(128)(2,1)S(1)}, bf16[2048]{0:T(1024)(128)(2,1)}, u32[]{:S(2)}) copy-start(bf16[2048]{0:T(1024)(128)(2,1)} %param.26) | copy-start | bytes 12292
  6.5 32.2 %copy-start.2 = (bf16[1,32,2048]{2,1,0:T(8,128)(2,1)S(1)}, bf16[1,32,2048]{2,1,0:T(8,128)(2,1)}, u32[]{:S(2)}) copy-start(bf16[1,32,2048]{2,1,0:T(8,128)(2,1)} %param.21) | copy-start | bytes 393220
  6.5 32.5 %copy-start.6 = (bf16[2,1024,8]{1,2,0:T(8,128)(2,1)S(1)}, bf16[2,1024,8]{1,2,0:T(8,128)(2,1)}, u32[]{:S(2)}) copy-start(bf16[2,1024,8]{1,2,0:T(8,128)(2,1)} %param.31) | copy-start | bytes 98308
  6.5 36.8 %copy-start.11 = (bf16[3,512]{1,0:T(4,128)(2,1)S(1)}, bf16[3,512]{1,0:T(4,128)(2,1)}, u32[]{:S(2)}) copy-start(bf16[3,512]{1,0:T(4,128)(2,1)} %param.32) | copy-start | bytes 9220
  6.5 36.8 %copy-start.17 = (bf16[3,128]{1,0:T(4,128)(2,1)S(1)}, bf16[3,128]{1,0:T(4,128)(2,1)}, u32[]{:S(2)}) copy-start(bf16[3,128]{1,0:T(4,128)(2,1)} %param.33) | copy-start | bytes 2308
  6.6 56.5 %all-gather.9.cloned.1.call-start = ((), (), s32[]{:S(2)}) async-start(), calls=%async_computation.1 | async-start | bytes 3145728 | tf_op jit(solution)/shard_map/all_gather | solution.py:173
  7.3 60.1 %all-gather.11.cloned.1.call-start = ((), (), s32[]{:S(2)}) async-start(), calls=%async_computation.2 | async-start | bytes 3145728 | tf_op jit(solution)/shard_map/all_gather | solution.py:176
  8.0 168.4 %all-reduce.3.cloned.1.call-start = ((), (), s32[]{:S(2)}) async-start(), calls=%async_computation.5 | async-start | bytes 1048576 | tf_op jit(solution)/shard_map/psum | solution.py:220
  8.8 54.2 %copy-start.20 = (f32[2,8]{1,0:T(2,128)S(1)}, f32[2,8]{1,0:T(2,128)}, u32[]{:S(2)}) copy-start(f32[2,8]{1,0:T(2,128)} %param.35) | copy-start | bytes 196
  77.5 14.1 %copy-start.5 = (bf16[1,640]{0,1:T(8,128)(2,1)S(1)}, bf16[1,640]{0,1:T(8,128)(2,1)}, u32[]{:S(2)}) copy-start(bf16[1,640]{0,1:T(8,128)(2,1)} %get-tuple-element.422) | copy-start | bytes 3844
  77.5 18.0 %copy-start.4 = (bf16[1,640]{0,1:T(8,128)(2,1)S(1)}, bf16[1,640]{0,1:T(8,128)(2,1)}, u32[]{:S(2)}) copy-start(bf16[1,640]{0,1:T(8,128)(2,1)} %get-tuple-element.423) | copy-start | bytes 3844
  77.5 19.4 %copy-start.24 = (pred[4]{0:T(512)(128)(4,1)S(1)}, pred[4]{0:T(512)(128)(4,1)}, u32[]{:S(2)}) copy-start(pred[4]{0:T(512)(128)(4,1)} %get-tuple-element.456) | copy-start | bytes 16
  77.6 25.3 %slice-start = ((bf16[128,656]{0,1:T(8,128)(2,1)}), bf16[128,640]{0,1:T(8,128)(2,1)S(1)}, s32[]{:S(2)}) async-start(bf16[128,656]{0,1:T(8,128)(2,1)} %copy-done.1), calls=%async_computation.6 | async-start | bytes 327680 | tf_op jit(solution)/shard_map/slice | solution.py:198
  91.7 6.7 %collective-permute-start.2 = (bf16[1,640]{0,1:T(8,128)(2,1)S(1)}, bf16[1,640]{0,1:T(8,128)(2,1)S(1)}, u32[]{:S(2)}, u32[]{:S(2)}) collective-permute-start(bf16[1,640]{0,1:T(8,128)(2,1)S(1)} %copy-done.5), channel_id=1, source_target_pairs={{0,8},{8,16},{16,24},{1,9},{9,17},{17,25},{2,10},{10,18},{18,26},{... | collective-permute-start | bytes 3848 | tf_op jit(solution)/shard_map/ppermute | solution.py:18
  95.6 7.2 %collective-permute-start.3 = (bf16[1,640]{0,1:T(8,128)(2,1)S(1)}, bf16[1,640]{0,1:T(8,128)(2,1)S(1)}, u32[]{:S(2)}, u32[]{:S(2)}) collective-permute-start(bf16[1,640]{0,1:T(8,128)(2,1)S(1)} %copy-done.4), channel_id=1, source_target_pairs={{8,0},{16,8},{24,16},{9,1},{17,9},{25,17},{10,2},{18,10},{26,18},{... | collective-permute-start | bytes 3848 | tf_op jit(solution)/shard_map/ppermute | solution.py:19
  97.1 10.3 %copy-start.18 = (bf16[3,128]{1,0:T(4,128)(2,1)S(1)}, bf16[3,128]{1,0:T(4,128)(2,1)}, u32[]{:S(2)}) copy-start(bf16[3,128]{1,0:T(4,128)(2,1)} %param.34) | copy-start | bytes 2308
  97.1 10.9 %copy-start.19 = (bf16[512]{0:T(512)(128)(2,1)S(1)}, bf16[512]{0:T(512)(128)(2,1)}, u32[]{:S(2)}) copy-start(bf16[512]{0:T(512)(128)(2,1)} %param.36) | copy-start | bytes 3076
  106.2 75.6 %all-gather.13.cloned.1.call-start = ((), (), s32[]{:S(2)}) async-start(), calls=%async_computation.3 | async-start | bytes 3145728 | tf_op jit(solution)/shard_map/all_gather | solution.py:179
  106.7 102.0 %reduce-scatter.2.cloned.1.call-start = ((), (), s32[]{:S(2)}) async-start(), calls=%async_computation.4 | async-start | bytes 655360 | tf_op jit(solution)/shard_map/reduce_scatter | solution.py:281
  111.0 27.5 %collective-permute-start = (bf16[1,768]{0,1:T(8,128)(2,1)S(1)}, bf16[1,768]{0,1:T(8,128)(2,1)S(1)}, u32[]{:S(2)}, u32[]{:S(2)}) collective-permute-start(bf16[1,768]{0,1:T(8,128)(2,1)S(1)} %get-tuple-element.416), channel_id=1, source_target_pairs={{0,8},{8,16},{16,24},{1,9},{9,17},{17,25},{2,10},{10,18},{18,26},{... | collective-permute-start | bytes 4616 | tf_op jit(solution)/shard_map/ppermute | solution.py:18
  113.0 25.5 %collective-permute-start.1 = (bf16[1,768]{0,1:T(8,128)(2,1)S(1)}, bf16[1,768]{0,1:T(8,128)(2,1)S(1)}, u32[]{:S(2)}, u32[]{:S(2)}) collective-permute-start(bf16[1,768]{0,1:T(8,128)(2,1)S(1)} %get-tuple-element.417), channel_id=1, source_target_pairs={{8,0},{16,8},{24,16},{9,1},{17,9},{25,17},{10,2},{18,10},{26,18},{... | collective-permute-start | bytes 4616 | tf_op jit(solution)/shard_map/ppermute | solution.py:19
  137.8 3.1 %copy-start.23 = (f32[8]{0:T(128)S(1)}, f32[8]{0:T(128)}, u32[]{:S(2)}) copy-start(f32[8]{0:T(128)} %exponential_multiply_fusion.1) | copy-start | bytes 100
  138.8 17.4 %copy-start.13 = (f32[1,8]{1,0:T(1,128)S(1)}, f32[1,8]{1,0:T(1,128)}, u32[]{:S(2)}) copy-start(f32[1,8]{1,0:T(1,128)} %custom-call) | copy-start | bytes 100
  138.8 17.4 %copy-start.15 = (bf16[4,1,8]{2,1,0:T(2,128)(2,1)S(1)}, bf16[4,1,8]{2,1,0:T(2,128)(2,1)}, u32[]{:S(2)}) copy-start(bf16[4,1,8]{2,1,0:T(2,128)(2,1)} %all_gather.58) | copy-start | bytes 196
  140.1 17.9 %copy-start.8 = (f32[128,8]{0,1:T(8,128)S(1)}, f32[128,8]{0,1:T(8,128)}, u32[]{:S(2)}) copy-start(f32[128,8]{0,1:T(8,128)} %get-tuple-element.448) | copy-start | bytes 12292
  140.1 18.0 %copy-start.22 = (f32[8]{0:T(128)S(1)}, f32[8]{0:T(128)}, u32[]{:S(2)}) copy-start(f32[8]{0:T(128)} %exponential_multiply_fusion) | copy-start | bytes 100
  140.8 33.2 %copy-start.12 = (f32[1,8]{1,0:T(1,128)S(1)}, f32[1,8]{1,0:T(1,128)}, u32[]{:S(2)}) copy-start(f32[1,8]{1,0:T(1,128)} %custom-call.2) | copy-start | bytes 100
  140.8 33.2 %copy-start.14 = (bf16[4,1,8]{2,1,0:T(2,128)(2,1)S(1)}, bf16[4,1,8]{2,1,0:T(2,128)(2,1)}, u32[]{:S(2)}) copy-start(bf16[4,1,8]{2,1,0:T(2,128)(2,1)} %all_gather.62) | copy-start | bytes 196
  156.8 19.6 %copy-start.7 = (f32[128,8]{0,1:T(8,128)S(1)}, f32[128,8]{0,1:T(8,128)}, u32[]{:S(2)}) copy-start(f32[128,8]{0,1:T(8,128)} %get-tuple-element.447) | copy-start | bytes 12292
  156.8 19.6 %copy-start.21 = (f32[8]{0:T(128)S(1)}, f32[8]{0:T(128)}, u32[]{:S(2)}) copy-start(f32[8]{0:T(128)} %get-tuple-element.426) | copy-start | bytes 100
  174.8 5.7 %copy-start.3 = (f32[128,512]{0,1:T(8,128)S(1)}, f32[128,512]{0,1:T(8,128)}, u32[]{:S(2)}) copy-start(f32[128,512]{0,1:T(8,128)} %get-tuple-element.418) | copy-start | bytes 786436
  (3 other events, 6.8 us)
Sparse Core Ops, SparseCore 0:
  8.9 13.3 all-gather.8
  23.8 11.7 all-gather.10
  106.3 40.7 all-reduce.2
  148.5 10.0 all-gather.12
  184.9 23.7 reduce-scatter.1
where the time goes:
time: 218 us; the launch traced here: 217 us
  blocking collectives  110 us (50%)
  waiting for transfers between devices  31.4 us (14%)
  matrix products  20.7 us (9%)
  other arithmetic  16.4 us (8%)
  local copies, waits for them, and re-layouts  15.9 us (7%)
  between operations  13.8 us (6%)
  starting transfers between devices  8.63 us (4%)
    all_gather x4, blocking collectives, carried_in_2(): lax.all_gather(part.astype(kind), axis)  51.8 us
    reduce_scatter x1, waiting for transfers between devices, shards(): lax.psum_scatter(jnp.dot(normed_out, full_out, preferred_element_type=jnp...  23.9 us
    psum x1, blocking collectives, shards(): summed = lax.psum(partial_value, 'sp')  20.4 us
    concatenate x1, local copies, waits for them, and re-layouts, shards(): jnp.concatenate([full_x, full_b, full_c, full_fwd, full_bwd, full_z], axi...  10.2 us
    all_gather x1, blocking collectives, shards(): lax.all_gather(latent_rows, 'tp', axis=0, tiled=True)  10 us
    all_gather x1, blocking collectives, shards(): mod_vectors = lax.all_gather(summed, 'tp', axis=2, tiled=True)  8.34 us
    all_gather x1, blocking collectives, shards(): lax.all_gather(jnp.stack([total_fwd, total_bwd])[None], 'sp', axis=0, til...  7.58 us
    ppermute x2, starting transfers between devices, with_halo(): before = lax.ppermute(last, axis, up)  5.86 us
  transfers between devices with their start and end apart: 9, of which 3 were waited for; matrix products, arithmetic and copies ran while one was open for 13% of the time, Pallas kernels for 0%

commit v1 on v0

--- a/solution.py
+++ b/solution.py
@@ -167,7 +167,11 @@
     partial_value = jnp.einsum(
         "ar,krc->kac", own_rows, mod_weight, preferred_element_type=jnp.float32
     )
-    summed = lax.psum(partial_value, "sp")
+    devices = lax.axis_size("sp")
+    summed, reach = (partial_value, 1)
+    while reach < devices:
+        summed = summed + lax.ppermute(summed, "sp", [(i_2, i_2 ^ reach) for i_2 in range(devices)])
+        reach = 2 * reach
     mod_vectors = lax.all_gather(summed, "tp", axis=2, tiled=True)
     full_x, full_b, full_c, full_z, full_fwd, full_bwd, full_out = (
         lax.all_gather(w_x, "dp", axis=0, tiled=True),

time: 218 us -> 198 us (0.908)
  blocking collectives: 110 us -> 85.3 us
  starting transfers between devices: 8.63 us -> 13.9 us
    psum x1 -> x0, blocking collectives: 20.4 us -> none  [shards(): summed = lax.psum(partial_value, 'sp')]
    ppermute x0 -> x2, starting transfers between devices: none -> 5.71 us  [shards(): lax.ppermute(summed, 'sp', [(i_2, i_2 ^ reach) for i_2 in range(devices)])]
  transfers between devices with their start and end apart: 9 -> 11, of which waited for: 3 -> 3; matrix products, arithmetic and copies ran while one was open for 13% -> 15% of each run, Pallas kernels for 0% -> 0%
where the time goes in v1:
time: 198 us; the launch traced here: 197 us
  blocking collectives  85.3 us (43%)
  waiting for transfers between devices  30.5 us (15%)
  matrix products  20.8 us (11%)
  local copies, waits for them, and re-layouts  17.4 us (9%)
  other arithmetic  15.5 us (8%)
  starting transfers between devices  13.9 us (7%)
  between operations  13.7 us (7%)
    all_gather x4, blocking collectives, carried_in_2(): lax.all_gather(part.astype(kind), axis)  50.4 us
    reduce_scatter x1, waiting for transfers between devices, shards(): lax.psum_scatter(jnp.dot(normed_out, full_out, preferred_element_type=jnp...  23.7 us
    all_gather x1, blocking collectives, shards(): lax.all_gather(latent_rows, 'tp', axis=0, tiled=True)  10.5 us
    concatenate x1, local copies, waits for them, and re-layouts, shards(): jnp.concatenate([full_x, full_b, full_c, full_fwd, full_bwd, full_z], axi...  10.2 us
    all_gather x1, blocking collectives, shards(): mod_vectors = lax.all_gather(summed, 'tp', axis=2, tiled=True)  8.39 us
    all_gather x1, blocking collectives, shards(): lax.all_gather(jnp.stack([total_fwd, total_bwd])[None], 'sp', axis=0, til...  8.01 us
    ppermute x2, starting transfers between devices, shards(): lax.ppermute(summed, 'sp', [(i_2, i_2 ^ reach) for i_2 in range(devices)])  5.71 us
    ppermute x2, starting transfers between devices, with_halo(): before = lax.ppermute(last, axis, up)  5.42 us
  transfers between devices with their start and end apart: 11, of which 3 were waited for; matrix products, arithmetic and copies ran while one was open for 15% of the time, Pallas kernels for 0%

profile of v1, /device:TPU:0, one launch (start us, length us, event | category | flops | bytes accessed | tf_op | source)
XLA Modules:
  0.0 197.4 jit_solution(15170654587870261484)
XLA Ops:
  9.3 3.1 %collective-permute-start = (f32[3,2,512]{2,1,0:T(2,128)S(1)}, f32[3,2,512]{2,1,0:T(2,128)S(1)}, u32[]{:S(2)}, u32[]{:S(2)}) collective-permute-start(f32[3,2,512]{2,1,0:T(2,128)S(1)} %convolution_bitcast_fusion.4), channel_id=1, source_target_pairs={{0,8},{8,0},{16,24},{24,16},{1,9},{9,1},{17,25},{25,17},{2,10},{10... | collective-permute-start | bytes 36872 | tf_op jit(solution)/shard_map/ppermute | solution.py:173
  12.6 2.2 %all_gather.53 = bf16[2048,128]{1,0:T(8,128)(2,1)S(1)} all-gather(bf16[1024,128]{1,0:T(8,128)(2,1)S(1)} %copy-done.4), channel_id=1, replica_groups=mesh['sp'=4,'tp'=4,'dp'=2] {'dp'}, dimensions={0}, use_global_device_ids=true | all-gather | bytes 786432 | tf_op jit(solution)/shard_map/all_gather | solution.py:178
  15.0 2.2 %all_gather.54 = bf16[2048,128]{1,0:T(8,128)(2,1)S(1)} all-gather(bf16[1024,128]{1,0:T(8,128)(2,1)S(1)} %copy-done.5), channel_id=1, replica_groups=mesh['sp'=4,'tp'=4,'dp'=2] {'dp'}, dimensions={0}, use_global_device_ids=true | all-gather | bytes 786432 | tf_op jit(solution)/shard_map/all_gather | solution.py:179
  17.7 2.7 %collective-permute-start.1 = (f32[3,2,512]{2,1,0:T(2,128)S(1)}, f32[3,2,512]{2,1,0:T(2,128)S(1)}, u32[]{:S(2)}, u32[]{:S(2)}) collective-permute-start(f32[3,2,512]{2,1,0:T(2,128)S(1)} %add.248), channel_id=1, source_target_pairs={{0,16},{8,24},{16,0},{24,8},{1,17},{9,25},{17,1},{25,9},{2,18},{10... | collective-permute-start | bytes 36872 | tf_op jit(solution)/shard_map/ppermute | solution.py:173
  20.3 1.8 all-gather
  22.2 1.0 copy.70
  23.2 1.8 all-gather.1
  25.0 1.0 copy.71
  26.1 8.4 %all_gather.50 = f32[3,2,2048]{2,1,0:T(2,128)S(1)} all-gather(f32[3,2,512]{2,1,0:T(2,128)S(1)} %add.249), channel_id=1, replica_groups=mesh['sp'=4,'tp'=4,'dp'=2] {'tp'}, dimensions={2}, use_global_device_ids=true | all-gather | bytes 61440 | tf_op jit(solution)/shard_map/all_gather | solution.py:175
  34.6 10.5 %all_gather.51 = bf16[128,2048]{1,0:T(8,128)(2,1)S(1)} all-gather(bf16[32,2048]{1,0:T(8,128)(2,1)S(1)} %fusion.46), channel_id=1, replica_groups=mesh['sp'=4,'tp'=4,'dp'=2] {'tp'}, dimensions={0}, use_global_device_ids=true | all-gather | bytes 655360 | tf_op jit(solution)/shard_map/all_gather | solution.py:233
  45.1 3.7 %fusion.16 = bf16[128,656]{0,1:T(8,128)(2,1)S(1)} fusion(bf16[2048,8]{1,0:T(8,128)(2,1)} %copy.71, bf16[2048,8]{1,0:T(8,128)(2,1)} %copy.70, bf16[2048,128]{1,0:T(8,128)(2,1)S(1)} %all_gather.53, bf16[2048,512]{1,0:T(8,128)(2,1)} %all-gather.9.cloned.1.call-done, bf16[1,128,2048]{2,1,0:T(8,128)(2,1)} %param.23, f32[2048]{0:T(1024)S(1)} %bitcast.220, ...), kind=kOutput, calls=%fused_computation.38 | convolution fusion | flops 356337664 | bytes 3404288 | tf_op jit(solution)/shard_map/dot_general | solution.py:198
  49.6 10.2 %concatenate.18 = bf16[2048,1296]{1,0:T(8,128)(2,1)} concatenate(bf16[2048,512]{1,0:T(8,128)(2,1)} %all-gather.9.cloned.1.call-done, bf16[2048,128]{1,0:T(8,128)(2,1)S(1)} %all_gather.53, bf16[2048,128]{1,0:T(8,128)(2,1)S(1)} %all_gather.54, bf16[2048,8]{1,0:T(8,128)(2,1)} %copy.70, bf16[2048,8]{1,0:T(8,128)(2,1)} %copy.71, bf16[2048,512]{1,0:T(8,128)(2,1)} %all-gather.11.cloned.1.call-done), dimensions={1} | concatenate | bytes 10616832 | tf_op jit(solution)/shard_map/concatenate | solution.py:193
  59.8 5.0 %convolution_convert_fusion.1 = bf16[128,1296]{0,1:T(8,128)(2,1)S(1)} fusion(bf16[128,2048]{1,0:T(8,128)(2,1)S(1)} %all_gather.51, bf16[2048,1296]{1,0:T(8,128)(2,1)} %concatenate.18), kind=kOutput, calls=%fused_computation.23 | convolution fusion | flops 679643136 | bytes 6164480 | tf_op jit(solution)/shard_map/dot_general | solution.py:232
  66.3 8.0 %all-gather.3 = f32[8,1,8]{2,1,0:T(1,128)S(1)} all-gather(f32[2,1,8]{2,1,0:T(1,128)S(1)} %pad_maximum_fusion.3), channel_id=5, replica_groups=mesh['sp'=4,'tp'=4,'dp'=2] {'sp'}, dimensions={0}, use_global_device_ids=true | all-gather | bytes 320 | tf_op jit(solution)/shard_map/all_gather | solution.py:215
  74.3 3.5 %collective-permute-start.4 = (bf16[1,640]{0,1:T(8,128)(2,1)S(1)}, bf16[1,640]{0,1:T(8,128)(2,1)S(1)}, u32[]{:S(2)}, u32[]{:S(2)}) collective-permute-start(bf16[1,640]{0,1:T(8,128)(2,1)S(1)} %copy-done.8), channel_id=1, source_target_pairs={{0,8},{8,16},{16,24},{1,9},{9,17},{17,25},{2,10},{10,18},{18,26},{... | collective-permute-start | bytes 3848 | tf_op jit(solution)/shard_map/ppermute | solution.py:18
  77.9 1.3 collective-permute-start.5
  79.5 1.1 collective-permute-done.4
  80.7 4.4 %collective-permute-done.5 = bf16[1,640]{0,1:T(8,128)(2,1)S(1)} collective-permute-done((bf16[1,640]{0,1:T(8,128)(2,1)S(1)}, bf16[1,640]{0,1:T(8,128)(2,1)S(1)}, u32[]{:S(2)}, u32[]{:S(2)}) %collective-permute-start.5) | collective-permute-done | bytes 1312 | tf_op jit(solution)/shard_map/ppermute | solution.py:19
  93.3 1.9 collective-permute-start.2
  95.2 1.3 collective-permute-start.3
  98.4 10.7 %all_gather.58 = bf16[4,1,8]{2,1,0:T(2,128)(2,1)} all-gather(bf16[1,1,8]{2,1,0:T(2,128)(2,1)S(1)} %slice.299), channel_id=1, replica_groups=mesh['sp'=4,'tp'=4,'dp'=2] {'sp'}, dimensions={0}, use_global_device_ids=true | all-gather | bytes 80 | tf_op jit(solution)/shard_map/all_gather | solution.py:27
  109.1 8.0 %all_gather.62 = bf16[4,1,8]{2,1,0:T(2,128)(2,1)} all-gather(bf16[1,1,8]{2,1,0:T(2,128)(2,1)S(1)} %slice.298), channel_id=1, replica_groups=mesh['sp'=4,'tp'=4,'dp'=2] {'sp'}, dimensions={0}, use_global_device_ids=true | all-gather | bytes 80 | tf_op jit(solution)/shard_map/all_gather | solution.py:27
  118.7 1.3 multiply_convert_fusion.2
  121.0 17.0 %all-gather.2 = bf16[32,64,128]{2,1,0:T(8,128)(2,1)S(1)} all-gather(bf16[8,64,128]{2,1,0:T(8,128)(2,1)S(1)} %fusion.21), channel_id=4, replica_groups=mesh['sp'=4,'tp'=4,'dp'=2] {'sp'}, dimensions={0}, use_global_device_ids=true | all-gather | bytes 655360 | tf_op jit(solution)/shard_map/all_gather | solution.py:27
  140.2 14.8 %all-gather.4 = bf16[32,64,128]{2,1,0:T(8,128)(2,1)S(1)} all-gather(bf16[8,64,128]{2,1,0:T(8,128)(2,1)S(1)} %fusion.22), channel_id=6, replica_groups=mesh['sp'=4,'tp'=4,'dp'=2] {'sp'}, dimensions={0}, use_global_device_ids=true | all-gather | bytes 655360 | tf_op jit(solution)/shard_map/all_gather | solution.py:27
  157.3 1.2 fusion.20
  158.5 1.2 fusion.13
  160.1 1.2 fusion.19
  161.3 1.2 fusion.15
  162.7 3.0 %convolution_convert_fusion = bf16[128,2048]{1,0:T(8,128)(2,1)} fusion(bf16[512,2048]{1,0:T(8,128)(2,1)} %all-gather.13.cloned.1.call-done, f32[128,512]{0,1:T(8,128)S(1)} %get-tuple-element.415, f32[512]{0:T(512)} %convert_element_type.388, f32[128]{0:T(128)S(1)} %add_rsqrt_fusion), kind=kOutput, calls=%fused_computation.22 | convolution fusion | flops 268894208 | bytes 2886144 | tf_op jit(solution)/shard_map/dot_general | solution.py:286
  165.7 23.7 %reduce-scatter.2.cloned.1.call-done = bf16[32,2048]{1,0:T(8,128)(2,1)} async-done(((bf16[128,2048]{1,0:T(8,128)(2,1)}), bf16[32,2048]{1,0:T(8,128)(2,1)}) %reduce-scatter.2.cloned.1.call-update) | async-done | bytes 131088 | tf_op jit(solution)/shard_map/reduce_scatter | solution.py:285
  189.3 1.6 fusion.71
  (194 shorter events, 25.0 us)
Async XLA Ops:
  6.5 6.0 %copy-start.4 = (bf16[1024,128]{1,0:T(8,128)(2,1)S(1)}, bf16[1024,128]{1,0:T(8,128)(2,1)}, u32[]{:S(2)}) copy-start(bf16[1024,128]{1,0:T(8,128)(2,1)} %param.28) | copy-start | bytes 786436
  6.5 8.2 %copy-start.23 = (f32[2,8]{1,0:T(2,128)S(1)}, f32[2,8]{1,0:T(2,128)}, u32[]{:S(2)}) copy-start(f32[2,8]{1,0:T(2,128)} %param.35) | copy-start | bytes 196
  6.5 8.2 %copy-start.2 = (bf16[1,128,2048]{2,1,0:T(8,128)(2,1)S(1)}, bf16[1,128,2048]{2,1,0:T(8,128)(2,1)}, u32[]{:S(2)}) copy-start(bf16[1,128,2048]{2,1,0:T(8,128)(2,1)} %param.23) | copy-start | bytes 1572868
  6.6 8.4 %copy-start.5 = (bf16[1024,128]{1,0:T(8,128)(2,1)S(1)}, bf16[1024,128]{1,0:T(8,128)(2,1)}, u32[]{:S(2)}) copy-start(bf16[1024,128]{1,0:T(8,128)(2,1)} %param.29) | copy-start | bytes 786436
  6.6 15.6 %copy-start.19 = (bf16[2048]{0:T(1024)(128)(2,1)S(1)}, bf16[2048]{0:T(1024)(128)(2,1)}, u32[]{:S(2)}) copy-start(bf16[2048]{0:T(1024)(128)(2,1)} %param.26) | copy-start | bytes 12292
  6.6 38.6 %all-gather.9.cloned.1.call-start = ((), (), s32[]{:S(2)}) async-start(), calls=%async_computation.1 | async-start | bytes 3145728 | tf_op jit(solution)/shard_map/all_gather | solution.py:177
  7.3 18.7 %copy-start.14 = (bf16[3,512]{1,0:T(4,128)(2,1)S(1)}, bf16[3,512]{1,0:T(4,128)(2,1)}, u32[]{:S(2)}) copy-start(bf16[3,512]{1,0:T(4,128)(2,1)} %param.32) | copy-start | bytes 9220
  7.3 18.7 %copy-start.20 = (bf16[3,128]{1,0:T(4,128)(2,1)S(1)}, bf16[3,128]{1,0:T(4,128)(2,1)}, u32[]{:S(2)}) copy-start(bf16[3,128]{1,0:T(4,128)(2,1)} %param.33) | copy-start | bytes 2308
  7.3 42.3 %all-gather.11.cloned.1.call-start = ((), (), s32[]{:S(2)}) async-start(), calls=%async_computation.2 | async-start | bytes 3145728 | tf_op jit(solution)/shard_map/all_gather | solution.py:180
  9.3 8.4 %collective-permute-start = (f32[3,2,512]{2,1,0:T(2,128)S(1)}, f32[3,2,512]{2,1,0:T(2,128)S(1)}, u32[]{:S(2)}, u32[]{:S(2)}) collective-permute-start(f32[3,2,512]{2,1,0:T(2,128)S(1)} %convolution_bitcast_fusion.4), channel_id=1, source_target_pairs={{0,8},{8,0},{16,24},{24,16},{1,9},{9,1},{17,25},{25,17},{2,10},{10... | collective-permute-start | bytes 36872 | tf_op jit(solution)/shard_map/ppermute | solution.py:173
  12.3 145.0 %all-reduce.3.cloned.1.call-start = ((), (), s32[]{:S(2)}) async-start(), calls=%async_computation.5 | async-start | bytes 1048576 | tf_op jit(solution)/shard_map/psum | solution.py:224
  17.7 8.4 %collective-permute-start.1 = (f32[3,2,512]{2,1,0:T(2,128)S(1)}, f32[3,2,512]{2,1,0:T(2,128)S(1)}, u32[]{:S(2)}, u32[]{:S(2)}) collective-permute-start(f32[3,2,512]{2,1,0:T(2,128)S(1)} %add.248), channel_id=1, source_target_pairs={{0,16},{8,24},{16,0},{24,8},{1,17},{9,25},{17,1},{25,9},{2,18},{10... | collective-permute-start | bytes 36872 | tf_op jit(solution)/shard_map/ppermute | solution.py:173
  59.8 14.5 %copy-start.8 = (bf16[1,640]{0,1:T(8,128)(2,1)S(1)}, bf16[1,640]{0,1:T(8,128)(2,1)}, u32[]{:S(2)}) copy-start(bf16[1,640]{0,1:T(8,128)(2,1)} %get-tuple-element.422) | copy-start | bytes 3844
  59.8 18.1 %copy-start.7 = (bf16[1,640]{0,1:T(8,128)(2,1)S(1)}, bf16[1,640]{0,1:T(8,128)(2,1)}, u32[]{:S(2)}) copy-start(bf16[1,640]{0,1:T(8,128)(2,1)} %get-tuple-element.423) | copy-start | bytes 3844
  59.8 19.4 %copy-start.27 = (pred[4]{0:T(512)(128)(4,1)S(1)}, pred[4]{0:T(512)(128)(4,1)}, u32[]{:S(2)}) copy-start(pred[4]{0:T(512)(128)(4,1)} %get-tuple-element.456) | copy-start | bytes 16
  59.8 25.3 %slice-start = ((bf16[128,656]{0,1:T(8,128)(2,1)}), bf16[128,640]{0,1:T(8,128)(2,1)S(1)}, s32[]{:S(2)}) async-start(bf16[128,656]{0,1:T(8,128)(2,1)} %copy-done.1), calls=%async_computation.6 | async-start | bytes 327680 | tf_op jit(solution)/shard_map/slice | solution.py:202
  74.3 6.3 %collective-permute-start.4 = (bf16[1,640]{0,1:T(8,128)(2,1)S(1)}, bf16[1,640]{0,1:T(8,128)(2,1)S(1)}, u32[]{:S(2)}, u32[]{:S(2)}) collective-permute-start(bf16[1,640]{0,1:T(8,128)(2,1)S(1)} %copy-done.8), channel_id=1, source_target_pairs={{0,8},{8,16},{16,24},{1,9},{9,17},{17,25},{2,10},{10,18},{18,26},{... | collective-permute-start | bytes 3848 | tf_op jit(solution)/shard_map/ppermute | solution.py:18
  77.9 7.2 %collective-permute-start.5 = (bf16[1,640]{0,1:T(8,128)(2,1)S(1)}, bf16[1,640]{0,1:T(8,128)(2,1)S(1)}, u32[]{:S(2)}, u32[]{:S(2)}) collective-permute-start(bf16[1,640]{0,1:T(8,128)(2,1)S(1)} %copy-done.7), channel_id=1, source_target_pairs={{8,0},{16,8},{24,16},{9,1},{17,9},{25,17},{10,2},{18,10},{26,18},{... | collective-permute-start | bytes 3848 | tf_op jit(solution)/shard_map/ppermute | solution.py:19
  79.4 10.3 %copy-start.21 = (bf16[3,128]{1,0:T(4,128)(2,1)S(1)}, bf16[3,128]{1,0:T(4,128)(2,1)}, u32[]{:S(2)}) copy-start(bf16[3,128]{1,0:T(4,128)(2,1)} %param.34) | copy-start | bytes 2308
  79.4 10.9 %copy-start.22 = (bf16[512]{0:T(512)(128)(2,1)S(1)}, bf16[512]{0:T(512)(128)(2,1)}, u32[]{:S(2)}) copy-start(bf16[512]{0:T(512)(128)(2,1)} %param.36) | copy-start | bytes 3076
  88.4 74.3 %all-gather.13.cloned.1.call-start = ((), (), s32[]{:S(2)}) async-start(), calls=%async_computation.3 | async-start | bytes 3145728 | tf_op jit(solution)/shard_map/all_gather | solution.py:183
  89.0 100.3 %reduce-scatter.2.cloned.1.call-start = ((), (), s32[]{:S(2)}) async-start(), calls=%async_computation.4 | async-start | bytes 655360 | tf_op jit(solution)/shard_map/reduce_scatter | solution.py:285
  93.3 25.1 %collective-permute-start.2 = (bf16[1,768]{0,1:T(8,128)(2,1)S(1)}, bf16[1,768]{0,1:T(8,128)(2,1)S(1)}, u32[]{:S(2)}, u32[]{:S(2)}) collective-permute-start(bf16[1,768]{0,1:T(8,128)(2,1)S(1)} %get-tuple-element.416), channel_id=1, source_target_pairs={{0,8},{8,16},{16,24},{1,9},{9,17},{17,25},{2,10},{10,18},{18,26},{... | collective-permute-start | bytes 4616 | tf_op jit(solution)/shard_map/ppermute | solution.py:18
  95.2 23.2 %collective-permute-start.3 = (bf16[1,768]{0,1:T(8,128)(2,1)S(1)}, bf16[1,768]{0,1:T(8,128)(2,1)S(1)}, u32[]{:S(2)}, u32[]{:S(2)}) collective-permute-start(bf16[1,768]{0,1:T(8,128)(2,1)S(1)} %get-tuple-element.417), channel_id=1, source_target_pairs={{8,0},{16,8},{24,16},{9,1},{17,9},{25,17},{10,2},{18,10},{26,18},{... | collective-permute-start | bytes 4616 | tf_op jit(solution)/shard_map/ppermute | solution.py:19
  118.7 19.4 %copy-start.16 = (f32[1,8]{1,0:T(1,128)S(1)}, f32[1,8]{1,0:T(1,128)}, u32[]{:S(2)}) copy-start(f32[1,8]{1,0:T(1,128)} %custom-call) | copy-start | bytes 100
  118.7 19.3 %copy-start.18 = (bf16[4,1,8]{2,1,0:T(2,128)(2,1)S(1)}, bf16[4,1,8]{2,1,0:T(2,128)(2,1)}, u32[]{:S(2)}) copy-start(bf16[4,1,8]{2,1,0:T(2,128)(2,1)} %all_gather.58) | copy-start | bytes 196
  120.0 19.9 %copy-start.11 = (f32[128,8]{0,1:T(8,128)S(1)}, f32[128,8]{0,1:T(8,128)}, u32[]{:S(2)}) copy-start(f32[128,8]{0,1:T(8,128)} %get-tuple-element.448) | copy-start | bytes 12292
  120.0 19.9 %copy-start.25 = (f32[8]{0:T(128)S(1)}, f32[8]{0:T(128)}, u32[]{:S(2)}) copy-start(f32[8]{0:T(128)} %exponential_multiply_fusion) | copy-start | bytes 100
  120.8 34.2 %copy-start.15 = (f32[1,8]{1,0:T(1,128)S(1)}, f32[1,8]{1,0:T(1,128)}, u32[]{:S(2)}) copy-start(f32[1,8]{1,0:T(1,128)} %custom-call.2) | copy-start | bytes 100
  120.8 34.2 %copy-start.17 = (bf16[4,1,8]{2,1,0:T(2,128)(2,1)S(1)}, bf16[4,1,8]{2,1,0:T(2,128)(2,1)}, u32[]{:S(2)}) copy-start(bf16[4,1,8]{2,1,0:T(2,128)(2,1)} %all_gather.62) | copy-start | bytes 196
  138.7 18.6 %copy-start.10 = (f32[128,8]{0,1:T(8,128)S(1)}, f32[128,8]{0,1:T(8,128)}, u32[]{:S(2)}) copy-start(f32[128,8]{0,1:T(8,128)} %get-tuple-element.447) | copy-start | bytes 12292
  138.7 18.6 %copy-start.24 = (f32[8]{0:T(128)S(1)}, f32[8]{0:T(128)}, u32[]{:S(2)}) copy-start(f32[8]{0:T(128)} %get-tuple-element.426) | copy-start | bytes 100
  (8 other events, 29.7 us)
Sparse Core Ops, SparseCore 0:
  8.9 13.2 all-gather.8
  23.8 11.7 all-gather.10
  88.5 39.7 all-reduce.2
  129.7 9.8 all-gather.12
  165.8 23.4 reduce-scatter.1
